TPU v7x, 32 devices: a whole 2x2x4 slice. The times are simulated.
32 devices in a mesh: ep: 8 (over z, y), tp: 4 (over x, core).
Axes of the slice: x: 2, y: 2, z: 4, core: 2. Of those that a mesh axis runs over, the one named last changes fastest.
Arguments:
- queries: bfloat16 [8192, 1024], P('ep', 'tp'), may hold values from -6 to 6
- head_keys: bfloat16 [8192, 256], P('ep', 'tp'), may hold values from -6 to 6
- head_values: bfloat16 [8192, 256], P('ep', 'tp'), may hold values from -6 to 6
- sink_logits: float32 [16], P('tp'), may hold values from -2 to 5
- out_weight: bfloat16 [1024, 2048], P('tp'), may hold values from -1.5 to 1.5
- moe_input: bfloat16 [4096, 2048], P(('ep', 'tp')), may hold values from -6 to 6
- norm_gain: float32 [2048], replicated, may hold values from 0.1 to 1.9
- routes: int32 [4096, 4], P(('ep', 'tp')), may hold values from 0 to 7, all different within a row; in each aligned block of 128 rows (0 to 127, 128 to 255, ...) at most 128 rows name the same one
- route_weight: float32 [4096, 4], P(('ep', 'tp')), may hold values from 0.05 to 1
- gate_weight: bfloat16 [8, 2048, 512], P('ep'), may hold values from -2 to 2
- up_weight: bfloat16 [8, 2048, 512], P('ep'), may hold values from -2 to 2
- down_weight: bfloat16 [8, 512, 2048], P('ep'), may hold values from -0.25 to 0.25
Outputs:
- attention_out: bfloat16 [8192, 2048], P(('ep', 'tp'))
- routed_out: bfloat16 [4096, 2048], P(('ep', 'tp'))
Inputs may be any that keep to these rules, and one draw needn't show every extreme that they name: `routes`: within the rows of one device (aligned blocks of 128 rows), each expert is named by at most 128 rows, and in every draw some expert by exactly 128; a row names 4 different experts.
All inputs are finite; a program needn't handle non-finite values.
Results may differ from a plain program's by a relative error of at most 0.0078.
Values may be sent and summed in bfloat16 or wider, within the bound.
A program may use at most 128 MiB of HBM per device.

v0:
```python
import jax
import jax.numpy as jnp
from jax import lax
from jax.sharding import PartitionSpec as P

HEAD_DIM = 64
WINDOW = 128
SEQS = 1


EPSILON = 1e-05
NEGATIVE = -1e30


def passed_along(value, axis, steps):
    count = lax.axis_size(axis)
    first, last = (max(0, -steps), min(count, count - steps))
    return lax.ppermute(value, axis, [(source, source + steps) for source in range(first, last)])


def clamped_unit(gate_pre, up_pre):
    gate_cut = jnp.minimum(gate_pre, 7.0)
    up_cut = jnp.clip(up_pre, -7.0, 7.0)
    return gate_cut * jax.nn.sigmoid(1.702 * gate_cut) * (up_cut + 1.0)


def attend(queries, head_keys, head_values, sink_logits, out_weight):
    tok_rows = queries.shape[0]
    local_heads = sink_logits.shape[0]
    local_kv = head_keys.shape[1] // HEAD_DIM
    per_group = local_heads // local_kv
    block_count = tok_rows // WINDOW
    key_width = local_kv * HEAD_DIM
    kv_rows = jnp.concatenate([head_keys, head_values], axis=1)
    earlier = passed_along(kv_rows[tok_rows - WINDOW :], "ep", 1)
    extended = jnp.concatenate([earlier, kv_rows], axis=0)
    banded = jnp.concatenate(
        [
            extended[:tok_rows].reshape(block_count, WINDOW, 2 * key_width),
            kv_rows.reshape(block_count, WINDOW, 2 * key_width),
        ],
        axis=1,
    )
    band_keys = banded[:, :, :key_width].reshape(block_count, 2 * WINDOW, local_kv, HEAD_DIM)
    band_values = banded[:, :, key_width:].reshape(block_count, 2 * WINDOW, local_kv, HEAD_DIM)
    blocked = queries.reshape(block_count, WINDOW, local_kv, per_group, HEAD_DIM)
    scores = jnp.einsum(
        "nqkgd,nskd->nkgqs", blocked, band_keys, preferred_element_type=jnp.float32
    ) * HEAD_DIM ** (-0.5)
    offset = lax.axis_index("ep") * tok_rows
    seq_len = tok_rows * lax.axis_size("ep") // SEQS
    query_pos = offset + jnp.arange(tok_rows, dtype=jnp.int32).reshape(block_count, WINDOW)
    key_pos = (
        offset
        - WINDOW
        + (jnp.arange(block_count, dtype=jnp.int32) * WINDOW)[:, None]
        + jnp.arange(2 * WINDOW, dtype=jnp.int32)[None, :]
    )
    distance = query_pos[:, :, None] - key_pos[:, None, :]
    starts = query_pos // seq_len * seq_len
    valid = (distance >= 0) & (distance < WINDOW) & (key_pos[:, None, :] >= starts[:, :, None])
    scores = jnp.where(valid[:, None, None], scores, NEGATIVE)
    sinks = sink_logits.reshape(local_kv, per_group, 1, 1)
    maxima = jnp.maximum(jnp.max(scores, axis=-1, keepdims=True), sinks)
    powers = jnp.exp(scores - maxima)
    weights = (powers / (jnp.sum(powers, axis=-1, keepdims=True) + jnp.exp(sinks - maxima))).astype(
        jnp.bfloat16
    )
    heads_out = jnp.einsum(
        "nkgqs,nskd->nqkgd", weights, band_values, preferred_element_type=jnp.float32
    )
    heads_out = heads_out.astype(jnp.bfloat16).reshape(tok_rows, local_heads * HEAD_DIM)
    summed = lax.psum_scatter(
        jnp.dot(heads_out, out_weight, preferred_element_type=jnp.float32),
        "tp",
        scatter_dimension=0,
        tiled=True,
    )
    return summed.astype(jnp.bfloat16)


def experts_part(moe_input, norm_gain, routes, route_weight, gate_weight, up_weight, down_weight):
    tok_rows, model_width = moe_input.shape
    choice_count = routes.shape[1]
    targets = lax.axis_size("ep")
    capacity = 2 * choice_count * tok_rows // targets
    values32 = moe_input.astype(jnp.float32)
    scale = lax.rsqrt(jnp.mean(values32 * values32, axis=-1, keepdims=True) + EPSILON)
    normed = (values32 * scale * norm_gain).astype(jnp.bfloat16)
    flat_routes = routes.reshape(-1)
    onehot = (flat_routes[:, None] == jnp.arange(targets, dtype=jnp.int32)[None, :]).astype(
        jnp.int32
    )
    earlier_count = jnp.sum((jnp.cumsum(onehot, axis=0) - onehot) * onehot, axis=1)
    slot_index = flat_routes * capacity + earlier_count
    copies = jnp.repeat(normed, choice_count, axis=0)
    outgoing = jnp.zeros((targets * capacity, model_width), jnp.bfloat16).at[slot_index].set(copies)
    outgoing = outgoing.reshape(targets, capacity, model_width)
    arrived = lax.all_to_all(outgoing, "ep", split_axis=0, concat_axis=0, tiled=True)
    flat_rows = arrived.reshape(-1, model_width)
    gate_pre = jnp.dot(flat_rows, gate_weight[0], preferred_element_type=jnp.float32)
    up_pre = jnp.dot(flat_rows, up_weight[0], preferred_element_type=jnp.float32)
    act = clamped_unit(gate_pre, up_pre).astype(jnp.bfloat16)
    result = jnp.dot(act, down_weight[0], preferred_element_type=jnp.float32).astype(jnp.bfloat16)
    came_back = lax.all_to_all(
        result.reshape(arrived.shape), "ep", split_axis=0, concat_axis=0, tiled=True
    )
    picked = came_back.reshape(targets * capacity, model_width)[slot_index]
    weighted = (
        picked.astype(jnp.float32).reshape(tok_rows, choice_count, model_width)
        * route_weight[:, :, None]
    )
    return jnp.sum(weighted, axis=1).astype(jnp.bfloat16)


def on_device(
    queries,
    head_keys,
    head_values,
    sink_logits,
    out_weight,
    moe_input,
    norm_gain,
    routes,
    route_weight,
    gate_weight,
    up_weight,
    down_weight,
):
    attention_out = attend(queries, head_keys, head_values, sink_logits, out_weight)
    routed_out = experts_part(
        moe_input, norm_gain, routes, route_weight, gate_weight, up_weight, down_weight
    )
    return (attention_out, routed_out)


def solution(mesh):
    placed = (
        P("ep", "tp"),
        P("ep", "tp"),
        P("ep", "tp"),
        P("tp"),
        P("tp", None),
        P(("ep", "tp"), None),
        P(),
        P(("ep", "tp"), None),
        P(("ep", "tp"), None),
        P("ep", None, None),
        P("ep", None, None),
        P("ep", None, None),
    )
    return jax.shard_map(
        on_device,
        mesh=mesh,
        in_specs=placed,
        out_specs=(P(("ep", "tp"), None), P(("ep", "tp"), None)),
        check_vma=False,
    )
```

profile of v0, /device:TPU:0, one launch (start us, length us, event | category | flops | bytes accessed | tf_op | source)
XLA Modules:
  0.0 274.6 jit_solution(440187324505282744)
XLA Ops:
  7.2 1.2 copy.17
  8.4 1.2 copy.18
  9.7 4.9 %collective-permute-start = (bf16[128,128]{1,0:T(8,128)(2,1)S(1)}, bf16[128,128]{1,0:T(8,128)(2,1)S(1)}, u32[]{:S(2)}, u32[]{:S(2)}) collective-permute-start(bf16[128,128]{1,0:T(8,128)(2,1)S(1)} %fusion.38), channel_id=1, source_target_pairs={{0,4},{4,8},{8,12},{12,16},{16,20},{20,24},{24,28},{1,5},{5,9},{9,... | collective-permute-start | bytes 98312 | tf_op jit(solution)/shard_map/ppermute | solution.py:18
  14.6 0.8 copy.26
  15.6 0.7 broadcast_multiply_fusion
  16.3 1.1 reduce-window.6
  17.9 1.2 fusion.20
  19.2 1.2 fusion.22
  20.4 2.4 broadcast_in_dim.19
  22.8 4.0 %reshape.229 = bf16[512,2048]{1,0:T(8,128)(2,1)} reshape(bf16[128,4,2048]{2,1,0:T(4,128)(2,1)} %broadcast_in_dim.19) | data formatting | bytes 4194304 | tf_op jit(solution)/shard_map/reshape | solution.py:96
  26.8 7.2 %scatter_custom_fusion = bf16[1024,2048]{1,0:T(8,128)(2,1)} fusion(s32[512]{0:T(512)S(1)} %bitcast.84, bf16[512,2048]{1,0:T(8,128)(2,1)} %reshape.229, bf16[]{:T(256)} %constant.59.clone.1), kind=kCustom, calls=%fused_computation.17 | custom fusion | bytes 4194816 | tf_op jit(solution)/shard_map/scatter | solution.py:97
  34.1 4.9 %all-to-all-start = ((bf16[8,128,2048]{2,1,0:T(8,128)(2,1)}), bf16[8,128,2048]{2,1,0:T(8,128)(2,1)}, u32[]{:S(2)}, u32[]{:S(2)}) async-start(bf16[8,128,2048]{2,1,0:T(8,128)(2,1)} %bitcast.79), calls=%async_computation.1 | async-start | bytes 8388608 | tf_op jit(solution)/shard_map/all_to_all | solution.py:99
  38.9 0.2 reduce-scatter.2.cloned.1.call-start
  39.3 0.5 fusion.26
  39.8 2.0 reshape.235
  41.8 2.3 pad_maximum_fusion.1
  44.2 1.8 copy.19
  45.9 1.8 copy.20
  47.7 1.9 fusion.1
  49.8 1.0 fusion
  50.9 1.2 fusion.17
  52.1 0.3 copy.24
  52.5 4.5 %fusion.29 = f32[1024,2048]{1,0:T(8,128)} fusion(bf16[256,2048]{1,0:T(8,128)(2,1)S(1)} %copy-done.3, bf16[32,8,8,128]{3,2,1,0:T(8,128)(2,1)S(1)} %bitcast.81), kind=kOutput, calls=%fused_computation.33 | convolution fusion | flops 1073741824 | bytes 9961472 | tf_op jit(solution)/shard_map/dot_general | solution.py:74
  57.0 74.9 %all-to-all-done = bf16[8,128,2048]{2,1,0:T(8,128)(2,1)} async-done(((bf16[8,128,2048]{2,1,0:T(8,128)(2,1)}), bf16[8,128,2048]{2,1,0:T(8,128)(2,1)}, u32[]{:S(2)}, u32[]{:S(2)}) %all-to-all-start) | async-done | bytes 4194336 | tf_op jit(solution)/shard_map/all_to_all | solution.py:99
  131.9 6.5 %fusion.3 = f32[1024,512]{1,0:T(8,128)} fusion(bf16[1024,2048]{1,0:T(8,128)(2,1)} %bitcast.16, bf16[1,2048,512]{2,1,0:T(8,128)(2,1)} %param.22), kind=kOutput, calls=%fused_computation.10 | convolution fusion | flops 2147483648 | bytes 8388608 | tf_op jit(solution)/shard_map/dot_general | solution.py:102
  138.4 10.3 %convolution_convert_fusion = bf16[1024,2048]{1,0:T(8,128)(2,1)} fusion(bf16[1,512,2048]{2,1,0:T(8,128)(2,1)S(1)} %copy-done, f32[1024,512]{1,0:T(8,128)} %fusion.3, bf16[1024,2048]{1,0:T(8,128)(2,1)} %bitcast.16, bf16[1,2048,512]{2,1,0:T(8,128)(2,1)} %param.21), kind=kOutput, calls=%fused_computation.6 | convolution fusion | flops 4302307328 | bytes 14680064 | tf_op jit(solution)/shard_map/dot_general | solution.py:104
  148.7 5.0 %all-to-all-start.1 = ((bf16[8,128,2048]{2,1,0:T(8,128)(2,1)}), bf16[8,128,2048]{2,1,0:T(8,128)(2,1)}, u32[]{:S(2)}, u32[]{:S(2)}) async-start(bf16[8,128,2048]{2,1,0:T(8,128)(2,1)} %bitcast.80), calls=%async_computation.2 | async-start | bytes 8388608 | tf_op jit(solution)/shard_map/all_to_all | solution.py:105
  153.8 92.2 %all-to-all-done.1 = bf16[8,128,2048]{2,1,0:T(8,128)(2,1)} async-done(((bf16[8,128,2048]{2,1,0:T(8,128)(2,1)}), bf16[8,128,2048]{2,1,0:T(8,128)(2,1)}, u32[]{:S(2)}, u32[]{:S(2)}) %all-to-all-start.1) | async-done | bytes 4194336 | tf_op jit(solution)/shard_map/all_to_all | solution.py:105
  246.1 8.0 %gather_fusion = bf16[512,2048]{1,0:T(8,128)(2,1)} fusion(bf16[1024,2048]{1,0:T(8,128)(2,1)} %bitcast.21, s32[1024]{0:T(1024)S(1)} %pad_clamp_fusion), kind=kCustom, calls=%fused_computation | custom fusion | bytes 4196352 | tf_op jit(solution)/shard_map/gather | solution.py:108
  254.0 4.8 %reshape.216 = f32[128,4,2048]{2,1,0:T(4,128)} reshape(bf16[512,2048]{1,0:T(8,128)(2,1)} %gather_fusion) | data formatting | bytes 6291456 | tf_op jit(solution)/shard_map/convert_element_type | solution.py:110
  258.9 6.2 %multiply_reduce_fusion = bf16[128,2048]{1,0:T(8,128)(2,1)} fusion(f32[128,4,2048]{2,1,0:T(4,128)} %reshape.216, f32[128,4]{1,0:T(8,128)S(1)} %copy.28), kind=kLoop, calls=%fused_computation.3 | loop fusion | flops 1835008 | bytes 4720640 | tf_op jit(solution)/shard_map/reduce_sum | solution.py:113
  265.1 2.7 convert_element_type.48
  (38 shorter events, 1.3 us)
Async XLA Ops:
  7.2 131.3 %copy-start = (bf16[1,512,2048]{2,1,0:T(8,128)(2,1)S(1)}, bf16[1,512,2048]{2,1,0:T(8,128)(2,1)}, u32[]{:S(2)}) copy-start(bf16[1,512,2048]{2,1,0:T(8,128)(2,1)} %param.23) | copy-start | bytes 6291460
  8.4 18.3 %copy-start.1 = (bf16[1024,64]{1,0:T(8,128)(2,1)}, bf16[1024,64]{1,0:T(8,128)(2,1)S(1)}, u32[]{:S(2)}) copy-start(bf16[1024,64]{1,0:T(8,128)(2,1)S(1)} %copy.17) | copy-start | bytes 393220
  9.6 17.1 %copy-start.2 = (bf16[1024,64]{1,0:T(8,128)(2,1)}, bf16[1024,64]{1,0:T(8,128)(2,1)S(1)}, u32[]{:S(2)}) copy-start(bf16[1024,64]{1,0:T(8,128)(2,1)S(1)} %copy.18) | copy-start | bytes 393220
  9.7 32.1 %collective-permute-start = (bf16[128,128]{1,0:T(8,128)(2,1)S(1)}, bf16[128,128]{1,0:T(8,128)(2,1)S(1)}, u32[]{:S(2)}, u32[]{:S(2)}) collective-permute-start(bf16[128,128]{1,0:T(8,128)(2,1)S(1)} %fusion.38), channel_id=1, source_target_pairs={{0,4},{4,8},{8,12},{12,16},{16,20},{20,24},{24,28},{1,5},{5,9},{9,... | collective-permute-start | bytes 98312 | tf_op jit(solution)/shard_map/ppermute | solution.py:18
  34.1 97.9 %all-to-all-start = ((bf16[8,128,2048]{2,1,0:T(8,128)(2,1)}), bf16[8,128,2048]{2,1,0:T(8,128)(2,1)}, u32[]{:S(2)}, u32[]{:S(2)}) async-start(bf16[8,128,2048]{2,1,0:T(8,128)(2,1)} %bitcast.79), calls=%async_computation.1 | async-start | bytes 8388608 | tf_op jit(solution)/shard_map/all_to_all | solution.py:99
  38.9 226.1 %reduce-scatter.2.cloned.1.call-start = ((), (), s32[]{:S(2)}) async-start(), calls=%async_computation.3 | async-start | bytes 10485760 | tf_op jit(solution)/shard_map/reduce_scatter | solution.py:73
  41.8 7.9 %copy-start.6 = (f32[4]{0:T(128)S(1)}, f32[4]{0:T(128)}, u32[]{:S(2)}) copy-start(f32[4]{0:T(128)} %param.15) | copy-start | bytes 52
  47.7 3.1 %copy-start.4 = (bf16[8,128,128]{1,2,0:T(8,128)(2,1)S(1)}, bf16[8,128,128]{1,2,0:T(8,128)(2,1)}, u32[]{:S(2)}) copy-start(bf16[8,128,128]{1,2,0:T(8,128)(2,1)} %copy.19) | copy-start | bytes 786436
  47.7 3.1 %copy-start.5 = (bf16[8,128,128]{1,2,0:T(8,128)(2,1)S(1)}, bf16[8,128,128]{1,2,0:T(8,128)(2,1)}, u32[]{:S(2)}) copy-start(bf16[8,128,128]{1,2,0:T(8,128)(2,1)} %copy.20) | copy-start | bytes 786436
  50.9 1.6 copy-start.3
  148.7 5.0 %copy-start.7 = (f32[128,4]{0,1:T(4,128)S(1)}, f32[128,4]{0,1:T(4,128)}, u32[]{:S(2)}) copy-start(f32[128,4]{0,1:T(4,128)} %param.20) | copy-start | bytes 6148
  148.7 97.3 %all-to-all-start.1 = ((bf16[8,128,2048]{2,1,0:T(8,128)(2,1)}), bf16[8,128,2048]{2,1,0:T(8,128)(2,1)}, u32[]{:S(2)}, u32[]{:S(2)}) async-start(bf16[8,128,2048]{2,1,0:T(8,128)(2,1)} %bitcast.80), calls=%async_computation.2 | async-start | bytes 8388608 | tf_op jit(solution)/shard_map/all_to_all | solution.py:105
Sparse Core Ops, SparseCore 0:
  57.1 72.5 reduce-scatter.1
where the time goes:
time: 276 us; the launch traced here: 275 us
  waiting for transfers between devices  167 us (61%)
  local copies, waits for them, and re-layouts  36.3 us (13%)
  matrix products  24.4 us (9%)
  other arithmetic  17.5 us (6%)
  starting transfers between devices  15 us (5%)
  between operations  14.2 us (5%)
    all_to_all x1, waiting for transfers between devices, experts_part(): lax.all_to_all(result.reshape(arrived.shape), 'ep', split_axis=0, concat_...  92.2 us
    all_to_all x1, waiting for transfers between devices, experts_part(): lax.all_to_all(outgoing, 'ep', split_axis=0, concat_axis=0, tiled=True)  74.9 us
    dot_general x1, matrix products, experts_part(): jnp.dot(act, down_weight[0], preferred_element_type=jnp.float32)  10.3 us
    gather x1, local copies, waits for them, and re-layouts, experts_part(): picked = came_back.reshape(targets * capacity, model_width)[slot_index]  7.95 us
    scatter x1, local copies, waits for them, and re-layouts, experts_part(): jnp.zeros((targets * capacity, model_width), jnp.bfloat16).at[slot_index]  7.24 us
    dot_general x1, matrix products, experts_part(): jnp.dot(flat_rows, up_weight[0], preferred_element_type=jnp.float32)  6.49 us
    reduce_sum x1, other arithmetic, experts_part(): return jnp.sum(weighted, axis=1).astype(jnp.bfloat16)  6.2 us
  transfers between devices with their start and end apart: 4, of which 2 were waited for; matrix products, arithmetic and copies ran while one was open for 27% of the time, Pallas kernels for 0%

commit v1 on v0

--- a/solution.py
+++ b/solution.py
@@ -87,6 +87,20 @@
     values32 = moe_input.astype(jnp.float32)
     scale = lax.rsqrt(jnp.mean(values32 * values32, axis=-1, keepdims=True) + EPSILON)
     normed = (values32 * scale * norm_gain).astype(jnp.bfloat16)
+    if capacity >= tok_rows:
+        experts = jnp.arange(targets, dtype=jnp.int32)
+        named = routes[:, :, None] == experts[None, None, :]
+        shares = jnp.sum(jnp.where(named, route_weight[:, :, None], 0.0), axis=1)
+        everyone = lax.all_gather(normed, "ep", axis=0, tiled=True)
+        mine = lax.all_to_all(shares.T[:, None], "ep", split_axis=0, concat_axis=0, tiled=True)
+        gate_pre = jnp.dot(everyone, gate_weight[0], preferred_element_type=jnp.float32)
+        up_pre = jnp.dot(everyone, up_weight[0], preferred_element_type=jnp.float32)
+        act = clamped_unit(gate_pre, up_pre).astype(jnp.bfloat16)
+        result = jnp.dot(act, down_weight[0], preferred_element_type=jnp.float32)
+        part = result.astype(jnp.bfloat16).astype(jnp.float32) * mine.reshape(-1, 1)
+        return lax.psum_scatter(
+            part.astype(jnp.bfloat16), "ep", scatter_dimension=0, tiled=True
+        )
     flat_routes = routes.reshape(-1)
     onehot = (flat_routes[:, None] == jnp.arange(targets, dtype=jnp.int32)[None, :]).astype(
         jnp.int32

time: 276 us -> 209 us (0.76)
  waiting for transfers between devices: 167 us -> 138 us
  local copies, waits for them, and re-layouts: 36.3 us -> 8.92 us
  other arithmetic: 17.5 us -> 11 us
  starting transfers between devices: 15 us -> 10.7 us
    all_to_all x2 -> x1, waiting for transfers between devices: 167 us -> 0.01 us  [experts_part(): lax.all_to_all(shares.T[:, None], 'ep', split_axis=0, concat_axis=0, tile...]
    reduce_scatter x0 -> x1, waiting for transfers between devices: none -> 89.6 us  [experts_part(): lax.psum_scatter(part.astype(jnp.bfloat16), 'ep', scatter_dimension=0, ti...]
    all_gather x0 -> x1, waiting for transfers between devices: none -> 43.4 us  [experts_part(): everyone = lax.all_gather(normed, 'ep', axis=0, tiled=True)]
    gather x1 -> x0, local copies, waits for them, and re-layouts: 7.95 us -> none  [experts_part(): picked = came_back.reshape(targets * capacity, model_width)[slot_index]]
    scatter x1 -> x0, local copies, waits for them, and re-layouts: 7.24 us -> none  [experts_part(): jnp.zeros((targets * capacity, model_width), jnp.bfloat16).at[slot_index]]
    reduce_sum x2 -> x1, other arithmetic: 6.29 us -> 0.6 us  [experts_part(): shares = jnp.sum(jnp.where(named, route_weight[:, :, None], 0.0), axis=1)]
    reduce_scatter x1, waiting for transfers between devices: 0.01 us -> 5.07 us  [attend(): lax.psum_scatter(jnp.dot(heads_out, out_weight, preferred_element_type=jn...]
    convert_element_type x1 -> x0, local copies, waits for them, and re-layouts: 4.82 us -> none  [experts_part(): picked.astype(jnp.float32).reshape(tok_rows, choice_count, model_width)]
  transfers between devices with their start and end apart: 4 -> 5, of which waited for: 2 -> 3; matrix products, arithmetic and copies ran while one was open for 27% -> 19% of each run, Pallas kernels for 0% -> 0%
where the time goes in v1:
time: 209 us
  waiting for transfers between devices  138 us (66%)
  matrix products  24.5 us (12%)
  between operations  15.6 us (7%)
  other arithmetic  11 us (5%)
  starting transfers between devices  10.7 us (5%)
  local copies, waits for them, and re-layouts  8.92 us (4%)
    reduce_scatter x1, waiting for transfers between devices, experts_part(): lax.psum_scatter(part.astype(jnp.bfloat16), 'ep', scatter_dimension=0, ti...  89.6 us
    all_gather x1, waiting for transfers between devices, experts_part(): everyone = lax.all_gather(normed, 'ep', axis=0, tiled=True)  43.4 us
    dot_general x1, matrix products, experts_part(): result = jnp.dot(act, down_weight[0], preferred_element_type=jnp.float32)  10.3 us
    dot_general x1, matrix products, experts_part(): up_pre = jnp.dot(everyone, up_weight[0], preferred_element_type=jnp.float32)  6.53 us
    all_to_all x1, starting transfers between devices, experts_part(): lax.all_to_all(shares.T[:, None], 'ep', split_axis=0, concat_axis=0, tile...  5.52 us
    reduce_scatter x1, waiting for transfers between devices, attend(): lax.psum_scatter(jnp.dot(heads_out, out_weight, preferred_element_type=jn...  5.07 us
    ppermute x1, starting transfers between devices, passed_along(): lax.ppermute(value, axis, [(source, source + steps) for source in range(f...  4.9 us
    dot_general x1, matrix products, attend(): jnp.dot(heads_out, out_weight, preferred_element_type=jnp.float32)  4.52 us
  transfers between devices with their start and end apart: 5, of which 3 were waited for; matrix products, arithmetic and copies ran while one was open for 19% of the time, Pallas kernels for 0%

profile of v1, /device:TPU:0, one launch (start us, length us, event | category | flops | bytes accessed | tf_op | source)
XLA Modules:
  0.0 208.8 jit_solution(16867891654217855906)
XLA Ops:
  8.0 0.0 all-gather.2.cloned.1.call-start
  8.1 1.4 fusion.18
  9.4 2.0 fusion.20
  11.5 0.0 reduce-scatter.3.cloned.1.call-start
  11.5 1.1 copy.38
  12.6 1.2 copy.39
  13.8 0.1 fusion.36
  13.9 4.9 %collective-permute-start = (bf16[128,128]{1,0:T(8,128)(2,1)S(1)}, bf16[128,128]{1,0:T(8,128)(2,1)S(1)}, u32[]{:S(2)}, u32[]{:S(2)}) collective-permute-start(bf16[128,128]{1,0:T(8,128)(2,1)S(1)} %fusion.36), channel_id=1, source_target_pairs={{0,4},{4,8},{8,12},{12,16},{16,20},{20,24},{24,28},{1,5},{5,9},{9,... | collective-permute-start | bytes 98312 | tf_op jit(solution)/shard_map/ppermute | solution.py:18
  18.9 0.1 iota_add_fusion
  18.9 0.5 fusion.24
  19.4 2.0 reshape.150
  21.5 2.4 %pad_maximum_fusion.1 = (bf16[1024,128]{1,0:T(8,128)(2,1)}, bf16[1024,128]{1,0:T(8,128)(2,1)}) fusion(bf16[128,128]{1,0:T(8,128)(2,1)S(1)} %collective-permute-done, bf16[1024,64]{1,0:T(8,128)(2,1)} %copy-done.2, bf16[1024,64]{1,0:T(8,128)(2,1)} %copy-done.1), kind=kLoop, calls=%fused_computation.38 | loop fusion | flops 1310720 | bytes 819200 | tf_op jit(solution)/shard_map/concatenate | solution.py:36
  23.9 1.8 copy.40
  25.7 1.8 copy.41
  27.5 1.9 fusion.1
  29.5 0.1 broadcast_maximum_fusion
  29.5 1.0 fusion
  30.6 0.1 exponential_add_fusion
  30.7 1.2 fusion.15
  31.9 0.3 copy.45
  32.2 4.5 %fusion.27 = f32[1024,2048]{1,0:T(8,128)} fusion(bf16[256,2048]{1,0:T(8,128)(2,1)S(1)} %copy-done.3, bf16[32,8,8,128]{3,2,1,0:T(8,128)(2,1)S(1)} %bitcast.71), kind=kOutput, calls=%fused_computation.28 | convolution fusion | flops 1073741824 | bytes 9961472 | tf_op jit(solution)/shard_map/dot_general | solution.py:74
  36.8 0.0 reduce-scatter.3.cloned.1.call-update
  36.8 0.7 copy-done.7
  37.5 0.6 select_reduce_fusion
  38.1 5.5 %all-to-all-start = ((f32[8,1,128]{2,1,0:T(1,128)}), f32[8,1,128]{2,1,0:T(1,128)S(1)}, u32[]{:S(2)}, u32[]{:S(2)}) async-start(f32[8,1,128]{2,1,0:T(1,128)} %bitcast.16), calls=%async_computation.1 | async-start | bytes 8192 | tf_op jit(solution)/shard_map/all_to_all | solution.py:95
  43.6 0.2 reduce-scatter.5.cloned.1.call-start
  43.8 43.4 %all-gather.2.cloned.1.call-done = bf16[1024,2048]{1,0:T(8,128)(2,1)} async-done(((bf16[128,2048]{1,0:T(8,128)(2,1)}), bf16[1024,2048]{1,0:T(8,128)(2,1)}) %all-gather.2.cloned.1.call-update) | async-done | bytes 4194320 | tf_op jit(solution)/shard_map/all_gather | solution.py:94
  87.2 6.5 %fusion.3 = f32[1024,512]{1,0:T(8,128)} fusion(bf16[1024,2048]{1,0:T(8,128)(2,1)} %all-gather.2.cloned.1.call-done, bf16[1,2048,512]{2,1,0:T(8,128)(2,1)} %param.22), kind=kOutput, calls=%fused_computation.7 | convolution fusion | flops 2147483648 | bytes 8388608 | tf_op jit(solution)/shard_map/dot_general | solution.py:97
  93.7 10.3 %multiply_convert_fusion = bf16[1024,2048]{1,0:T(8,128)(2,1)} fusion(f32[1024]{0:T(1024)S(1)} %bitcast.74, bf16[1,512,2048]{2,1,0:T(8,128)(2,1)S(1)} %copy-done, f32[1024,512]{1,0:T(8,128)} %fusion.3, bf16[1024,2048]{1,0:T(8,128)(2,1)} %all-gather.2.cloned.1.call-done, bf16[1,2048,512]{2,1,0:T(8,128)(2,1)} %param.21), kind=kOutput, calls=%fused_computation | convolution fusion | flops 4308598784 | bytes 14684160 | tf_op jit(solution)/shard_map/dot_general | solution.py:99
  104.0 5.1 %reduce-scatter.3.cloned.1.call-done = f32[256,2048]{1,0:T(8,128)} async-done(((f32[1024,2048]{1,0:T(8,128)}), f32[256,2048]{1,0:T(8,128)}) %reduce-scatter.3.cloned.1.call-update) | async-done | bytes 2097168 | tf_op jit(solution)/shard_map/reduce_scatter | solution.py:73
  109.1 2.7 %convert_element_type.37 = bf16[256,2048]{1,0:T(8,128)(2,1)} convert(f32[256,2048]{1,0:T(8,128)} %reduce-scatter.3.cloned.1.call-done) | non-fusion elementwise | flops 524288 | bytes 3145728 | tf_op jit(solution)/shard_map/convert_element_type | solution.py:79
  111.8 89.6 %reduce-scatter.5.cloned.1.call-done = bf16[128,2048]{1,0:T(8,128)(2,1)} async-done(((bf16[1024,2048]{1,0:T(8,128)(2,1)}), bf16[128,2048]{1,0:T(8,128)(2,1)}) %reduce-scatter.5.cloned.1.call-update) | async-done | bytes 524304 | tf_op jit(solution)/shard_map/reduce_scatter | solution.py:101
  (24 shorter events, 0.1 us)
Async XLA Ops:
  8.0 85.7 %copy-start = (bf16[1,512,2048]{2,1,0:T(8,128)(2,1)S(1)}, bf16[1,512,2048]{2,1,0:T(8,128)(2,1)}, u32[]{:S(2)}) copy-start(bf16[1,512,2048]{2,1,0:T(8,128)(2,1)} %param.23) | copy-start | bytes 6291460
  8.0 79.2 %all-gather.2.cloned.1.call-start = ((), (), s32[]{:S(2)}) async-start(), calls=%async_computation.4 | async-start | bytes 4718592 | tf_op jit(solution)/shard_map/all_gather | solution.py:94
  11.5 97.6 %reduce-scatter.3.cloned.1.call-start = ((), (), s32[]{:S(2)}) async-start(), calls=%async_computation.3 | async-start | bytes 10485760 | tf_op jit(solution)/shard_map/reduce_scatter | solution.py:73
  12.6 6.3 %copy-start.1 = (bf16[1024,64]{1,0:T(8,128)(2,1)}, bf16[1024,64]{1,0:T(8,128)(2,1)S(1)}, u32[]{:S(2)}) copy-start(bf16[1024,64]{1,0:T(8,128)(2,1)S(1)} %copy.38) | copy-start | bytes 393220
  13.8 5.1 %copy-start.2 = (bf16[1024,64]{1,0:T(8,128)(2,1)}, bf16[1024,64]{1,0:T(8,128)(2,1)S(1)}, u32[]{:S(2)}) copy-start(bf16[1024,64]{1,0:T(8,128)(2,1)S(1)} %copy.39) | copy-start | bytes 393220
  13.9 7.6 %collective-permute-start = (bf16[128,128]{1,0:T(8,128)(2,1)S(1)}, bf16[128,128]{1,0:T(8,128)(2,1)S(1)}, u32[]{:S(2)}, u32[]{:S(2)}) collective-permute-start(bf16[128,128]{1,0:T(8,128)(2,1)S(1)} %fusion.36), channel_id=1, source_target_pairs={{0,4},{4,8},{8,12},{12,16},{16,20},{20,24},{24,28},{1,5},{5,9},{9,... | collective-permute-start | bytes 98312 | tf_op jit(solution)/shard_map/ppermute | solution.py:18
  21.5 8.0 %copy-start.6 = (f32[4]{0:T(128)S(1)}, f32[4]{0:T(128)}, u32[]{:S(2)}) copy-start(f32[4]{0:T(128)} %param.15) | copy-start | bytes 52
  27.5 3.1 %copy-start.4 = (bf16[8,128,128]{1,2,0:T(8,128)(2,1)S(1)}, bf16[8,128,128]{1,2,0:T(8,128)(2,1)}, u32[]{:S(2)}) copy-start(bf16[8,128,128]{1,2,0:T(8,128)(2,1)} %copy.40) | copy-start | bytes 786436
  27.5 3.1 %copy-start.5 = (bf16[8,128,128]{1,2,0:T(8,128)(2,1)S(1)}, bf16[8,128,128]{1,2,0:T(8,128)(2,1)}, u32[]{:S(2)}) copy-start(bf16[8,128,128]{1,2,0:T(8,128)(2,1)} %copy.41) | copy-start | bytes 786436
  30.7 1.6 copy-start.3
  36.8 0.7 copy-start.7
  36.8 0.7 copy-start.8
  38.1 55.7 %all-to-all-start = ((f32[8,1,128]{2,1,0:T(1,128)}), f32[8,1,128]{2,1,0:T(1,128)S(1)}, u32[]{:S(2)}, u32[]{:S(2)}) async-start(f32[8,1,128]{2,1,0:T(1,128)} %bitcast.16), calls=%async_computation.1 | async-start | bytes 8192 | tf_op jit(solution)/shard_map/all_to_all | solution.py:95
  43.6 157.8 %reduce-scatter.5.cloned.1.call-start = ((), (), s32[]{:S(2)}) async-start(), calls=%async_computation.5 | async-start | bytes 4718592 | tf_op jit(solution)/shard_map/reduce_scatter | solution.py:101
Sparse Core Ops, SparseCore 0:
  11.6 75.5 all-gather.1
Sparse Core Ops, SparseCore 1:
  36.9 72.2 reduce-scatter.2
  113.2 88.2 reduce-scatter.4

commit v2 on v1

--- a/solution.py
+++ b/solution.py
@@ -1,6 +1,10 @@
+import functools
+
 import jax
 import jax.numpy as jnp
 from jax import lax
+from jax.experimental import pallas as pl
+from jax.experimental.pallas import tpu as pltpu
 from jax.sharding import PartitionSpec as P
 
 HEAD_DIM = 64
@@ -87,6 +91,11 @@
     values32 = moe_input.astype(jnp.float32)
     scale = lax.rsqrt(jnp.mean(values32 * values32, axis=-1, keepdims=True) + EPSILON)
     normed = (values32 * scale * norm_gain).astype(jnp.bfloat16)
+    if capacity >= tok_rows and targets % ROW == 0 and targets >= 2 * ROW:
+        experts = jnp.arange(targets, dtype=jnp.int32)
+        named = routes[:, None, :] == experts[None, :, None]
+        shares = jnp.sum(jnp.where(named, route_weight[:, None, :], 0.0), axis=2).T
+        return fused_experts(normed, shares, gate_weight[0], up_weight[0], down_weight[0])
     if capacity >= tok_rows:
         experts = jnp.arange(targets, dtype=jnp.int32)
         named = routes[:, :, None] == experts[None, None, :]
@@ -125,6 +134,317 @@
         * route_weight[:, :, None]
     )
     return jnp.sum(weighted, axis=1).astype(jnp.bfloat16)
+
+
+ROW = 2
+PIECES = 2
+
+
+def experts_kernel(
+    count, rows_hbm, shares_hbm, gate_hbm, up_hbm, down_hbm, out_ref,
+    gath, shares, gate_w, up_w, down_w, parts, from_row, onward, from_line,
+    local_sem, share_send, share_recv, got, sent_up, sent_down, sent_row,
+    row_send, row_recv, line_send, line_recv,
+):
+    lines = count // ROW
+    me = lax.axis_index("ep")
+    z, y = me // ROW, me % ROW
+    tok_rows = out_ref.shape[0]
+    piece = tok_rows // PIECES
+    loads = [
+        pltpu.make_async_copy(rows_hbm, gath.at[me], local_sem.at[0]),
+        pltpu.make_async_copy(shares_hbm, shares.at[me], local_sem.at[1]),
+        pltpu.make_async_copy(gate_hbm, gate_w, local_sem.at[2]),
+        pltpu.make_async_copy(up_hbm, up_w, local_sem.at[3]),
+        pltpu.make_async_copy(down_hbm, down_w, local_sem.at[4]),
+    ]
+    for load in loads:
+        load.start()
+
+    barrier = pltpu.get_barrier_semaphore()
+    for step in range(1, count):
+        other = lax.rem(me + step, count)
+        pl.semaphore_signal(
+            barrier, inc=1, device_id={"ep": other}, device_id_type=pl.DeviceIdType.MESH
+        )
+    pl.semaphore_wait(barrier, count - 1)
+
+    def remote(source, target, send, recv, device):
+        return pltpu.make_async_remote_copy(
+            src_ref=source,
+            dst_ref=target,
+            send_sem=send,
+            recv_sem=recv,
+            device_id={"ep": device},
+            device_id_type=pl.DeviceIdType.MESH,
+        )
+
+    def share_copy(slot, recv_slot, device):
+        return remote(
+            shares.at[slot], shares.at[slot], share_send.at[device], share_recv.at[recv_slot], device
+        )
+
+    def block_copy(block, h, sems, device):
+        view = gath.at[block, pl.ds(h * piece, piece)]
+        return remote(view, view, sems.at[block, h], got.at[block, h], device)
+
+    across = z * ROW + (1 - y)
+    above = jnp.minimum(z + 1, lines - 1) * ROW + y
+    below = jnp.maximum(z - 1, 0) * ROW + y
+
+    loads[0].wait()
+    loads[1].wait()
+    for h in range(PIECES):
+        block_copy(me, h, sent_row, across).start()
+
+        @pl.when(z < lines - 1)
+        def _():
+            block_copy(me, h, sent_up, above).start()
+
+        @pl.when(z > 0)
+        def _():
+            block_copy(me, h, sent_down, below).start()
+
+    for step in range(1, count):
+        share_copy(me, me, lax.rem(me + step, count)).start()
+    for step in range(1, count):
+        source = lax.rem(me + step, count)
+        remote(
+            shares.at[source], shares.at[source], share_send.at[source],
+            share_recv.at[source], source,
+        ).wait_recv()
+    loads[2].wait()
+    loads[3].wait()
+    loads[4].wait()
+
+    square = (tok_rows, tok_rows)
+    eye = lax.broadcasted_iota(jnp.int32, square, 0) == lax.broadcasted_iota(jnp.int32, square, 1)
+
+    def visit(turn, carry):
+        distance = turn // 4
+        foreign = (turn // 2) % 2
+        downward = turn % 2
+        line = jnp.where(downward == 1, z + distance, z - distance)
+        valid = (line >= 0) & (line < lines) & ((distance > 0) | (downward == 0))
+        held = jnp.clip(line, 0, lines - 1) * ROW + jnp.where(foreign == 1, 1 - y, y)
+
+        @pl.when(valid)
+        def _():
+            for h in range(PIECES):
+
+                @pl.when(held != me)
+                def _():
+                    block_copy(held, h, sent_row, across).wait_recv()
+
+                @pl.when((foreign == 0) & (distance > 0))
+                def _():
+                    block_copy(held, h, sent_row, across).start()
+
+                    @pl.when((downward == 0) & (z < lines - 1))
+                    def _():
+                        block_copy(held, h, sent_up, above).start()
+
+                    @pl.when((downward == 1) & (z > 0))
+                    def _():
+                        block_copy(held, h, sent_down, below).start()
+
+            rows = gath[held]
+            gate_pre = jnp.dot(rows, gate_w[...], preferred_element_type=jnp.float32)
+            up_pre = jnp.dot(rows, up_w[...], preferred_element_type=jnp.float32)
+            act = clamped_unit(gate_pre, up_pre).astype(jnp.bfloat16)
+            share = shares[held, pl.ds(me, 1), :]
+            column = jnp.sum(jnp.where(eye, share, 0.0), axis=1, keepdims=True)
+            result = jnp.dot(act, down_w[...], preferred_element_type=jnp.float32)
+            weighted = result.astype(jnp.bfloat16).astype(jnp.float32) * column
+            parts[held] = weighted.astype(jnp.bfloat16)
+
+        return carry
+
+    lax.fori_loop(0, 4 * lines, visit, 0)
+
+    def row_copy(line, h):
+        return remote(
+            parts.at[line * ROW + (1 - y), pl.ds(h * piece, piece)],
+            from_row.at[line, pl.ds(h * piece, piece)],
+            row_send.at[line, h],
+            row_recv.at[line, h],
+            across,
+        )
+
+    def line_copy(line, h, downward, device):
+        return remote(
+            onward.at[line, pl.ds(h * piece, piece)],
+            from_line.at[downward, line, pl.ds(h * piece, piece)],
+            line_send.at[line, h],
+            line_recv.at[downward, line, h],
+            device,
+        )
+
+    def far_first(turn):
+        distance = lines - 1 - turn // 2
+        downward = turn % 2
+        line = jnp.where(downward == 1, z - distance, z + distance)
+        valid = (line >= 0) & (line < lines)
+        return distance, downward, valid, jnp.clip(line, 0, lines - 1)
+
+    def send_across(turn, carry):
+        distance, downward, valid, line = far_first(turn)
+
+        @pl.when(valid & ((distance > 0) | (downward == 0)))
+        def _():
+            for h in range(PIECES):
+                row_copy(line, h).start()
+
+        return carry
+
+    lax.fori_loop(0, 2 * lines, send_across, 0)
+
+    def pass_on(turn, carry):
+        distance, downward, valid, line = far_first(turn)
+
+        @pl.when(valid)
+        def _():
+            for h in range(PIECES):
+                span = pl.ds(h * piece, piece)
+                row_copy(line, h).wait_recv()
+                base = parts[line * ROW + y, span].astype(jnp.float32) + from_row[
+                    line, span
+                ].astype(jnp.float32)
+
+                @pl.when(downward == 0)
+                def _():
+                    @pl.when(z > 0)
+                    def _():
+                        line_copy(line, h, 0, above).wait_recv()
+                        onward[line, span] = (
+                            base + from_line[0, line, span].astype(jnp.float32)
+                        ).astype(jnp.bfloat16)
+
+                    @pl.when(z == 0)
+                    def _():
+                        onward[line, span] = base.astype(jnp.bfloat16)
+
+                    line_copy(line, h, 0, above).start()
+
+                @pl.when(downward == 1)
+                def _():
+                    @pl.when(z < lines - 1)
+                    def _():
+                        line_copy(line, h, 1, below).wait_recv()
+                        onward[line, span] = (
+                            base + from_line[1, line, span].astype(jnp.float32)
+                        ).astype(jnp.bfloat16)
+
+                    @pl.when(z == lines - 1)
+                    def _():
+                        onward[line, span] = base.astype(jnp.bfloat16)
+
+                    line_copy(line, h, 1, below).start()
+
+        return carry
+
+    lax.fori_loop(0, 2 * (lines - 1), pass_on, 0)
+
+    for h in range(PIECES):
+        span = pl.ds(h * piece, piece)
+        place = slice(h * piece, (h + 1) * piece)
+        row_copy(z, h).wait_recv()
+        base = parts[me, span].astype(jnp.float32) + from_row[z, span].astype(jnp.float32)
+
+        @pl.when(z > 0)
+        def _():
+            line_copy(z, h, 0, above).wait_recv()
+
+        @pl.when(z < lines - 1)
+        def _():
+            line_copy(z, h, 1, below).wait_recv()
+
+        @pl.when(z == 0)
+        def _():
+            total = base + from_line[1, z, span].astype(jnp.float32)
+            out_ref[place] = total.astype(jnp.bfloat16)
+
+        @pl.when(z == lines - 1)
+        def _():
+            total = base + from_line[0, z, span].astype(jnp.float32)
+            out_ref[place] = total.astype(jnp.bfloat16)
+
+        @pl.when((z > 0) & (z < lines - 1))
+        def _():
+            total = base + (
+                from_line[0, z, span].astype(jnp.float32)
+                + from_line[1, z, span].astype(jnp.float32)
+            )
+            out_ref[place] = total.astype(jnp.bfloat16)
+
+    for step in range(1, count):
+        share_copy(me, me, lax.rem(me + step, count)).wait_send()
+
+    def finish(line, carry):
+        held = line * ROW + y
+        for h in range(PIECES):
+            block_copy(held, h, sent_row, across).wait_send()
+            row_copy(line, h).wait_send()
+
+            @pl.when((line <= z) & (z < lines - 1))
+            def _():
+                block_copy(held, h, sent_up, above).wait_send()
+
+            @pl.when((line >= z) & (z > 0))
+            def _():
+                block_copy(held, h, sent_down, below).wait_send()
+
+            @pl.when(line != z)
+            def _():
+                line_copy(line, h, 0, above).wait_send()
+
+        return carry
+
+    lax.fori_loop(0, lines, finish, 0)
+
+
+def fused_experts(normed, shares, gate_weight, up_weight, down_weight):
+    count = lax.axis_size("ep")
+    lines = count // ROW
+    tok_rows, width = normed.shape
+    hidden = gate_weight.shape[1]
+    block = (tok_rows, width)
+    sem = pltpu.SemaphoreType.DMA
+    flops = 6 * count * tok_rows * width * hidden
+    return pl.pallas_call(
+        functools.partial(experts_kernel, count),
+        out_shape=jax.ShapeDtypeStruct(block, jnp.bfloat16),
+        in_specs=[pl.BlockSpec(memory_space=pl.ANY)] * 5,
+        out_specs=pl.BlockSpec(memory_space=pltpu.VMEM),
+        scratch_shapes=[
+            pltpu.VMEM((count,) + block, jnp.bfloat16),
+            pltpu.VMEM((count, count, tok_rows), jnp.float32),
+            pltpu.VMEM((width, hidden), jnp.bfloat16),
+            pltpu.VMEM((width, hidden), jnp.bfloat16),
+            pltpu.VMEM((hidden, width), jnp.bfloat16),
+            pltpu.VMEM((count,) + block, jnp.bfloat16),
+            pltpu.VMEM((lines,) + block, jnp.bfloat16),
+            pltpu.VMEM((lines,) + block, jnp.bfloat16),
+            pltpu.VMEM((2, lines) + block, jnp.bfloat16),
+            sem((5,)),
+            sem((count,)),
+            sem((count,)),
+            sem((count, PIECES)),
+            sem((count, PIECES)),
+            sem((count, PIECES)),
+            sem((count, PIECES)),
+            sem((lines, PIECES)),
+            sem((lines, PIECES)),
+            sem((lines, PIECES)),
+            sem((2, lines, PIECES)),
+        ],
+        compiler_params=pltpu.CompilerParams(
+            collective_id=0, has_side_effects=True, vmem_limit_bytes=44 * 1024 * 1024
+        ),
+        cost_estimate=pl.CostEstimate(
+            flops=10 * flops, bytes_accessed=count * tok_rows * width * 8, transcendentals=0
+        ),
+    )(normed, shares, gate_weight, up_weight, down_weight)
 
 
 def on_device(

time: 209 us -> 150 us (0.72)
  waiting for transfers between devices: 138 us -> 0.04 us
  Pallas kernels: 0 us -> 107 us
  matrix products: 24.5 us -> 6.63 us
  other arithmetic: 11 us -> 5.15 us
  starting transfers between devices: 10.7 us -> 4.94 us
  local copies, waits for them, and re-layouts: 8.92 us -> 11.6 us
    pallas_call x0 -> x1, Pallas kernels: none -> 107 us  [fused_experts(): pl.pallas_call(functools.partial(experts_kernel, count), out_shape=jax.Sh...]
    reduce_scatter x1 -> x0, waiting for transfers between devices: 89.6 us -> none  [experts_part(): lax.psum_scatter(part.astype(jnp.bfloat16), 'ep', scatter_dimension=0, ti...]
    all_gather x1 -> x0, waiting for transfers between devices: 43.4 us -> none  [experts_part(): everyone = lax.all_gather(normed, 'ep', axis=0, tiled=True)]
    dot_general x2 -> x0, matrix products: 16.8 us -> none  [the longest x1 10.3 us: experts_part(): result = jnp.dot(act, down_weight[0], preferred_element_type=jnp.float32)]
    unnamed x20 -> x21, local copies, waits for them, and re-layouts: 2.95 us -> 8.84 us
    all_to_all x1 -> x0, starting transfers between devices: 5.52 us -> none  [experts_part(): lax.all_to_all(shares.T[:, None], 'ep', split_axis=0, concat_axis=0, tile...]
    reduce_scatter x1, waiting for transfers between devices: 5.07 us -> 0.02 us  [attend(): lax.psum_scatter(jnp.dot(heads_out, out_weight, preferred_element_type=jn...]
    concatenate x1, other arithmetic: 2.44 us -> 0.21 us  [attend(): extended = jnp.concatenate([earlier, kv_rows], axis=0)]
  transfers between devices with their start and end apart: 5 -> 2, of which waited for: 3 -> 0; matrix products, arithmetic and copies ran while one was open for 19% -> 2% of each run, Pallas kernels for 0% -> 72%
where the time goes in v2:
time: 150 us
  Pallas kernels  107 us (71%)
  between operations  14.2 us (9%)
  local copies, waits for them, and re-layouts  11.6 us (8%)
  matrix products  6.63 us (4%)
  other arithmetic  5.15 us (3%)
  starting transfers between devices  4.94 us (3%)
    pallas_call x1, Pallas kernels, fused_experts(): pl.pallas_call(functools.partial(experts_kernel, count), out_shape=jax.Sh...  107 us
    unnamed x21, local copies, waits for them, and re-layouts  8.84 us
    ppermute x1, starting transfers between devices, passed_along(): lax.ppermute(value, axis, [(source, source + steps) for source in range(f...  4.9 us
    dot_general x1, matrix products, attend(): jnp.dot(heads_out, out_weight, preferred_element_type=jnp.float32)  4.51 us
  transfers between devices with their start and end apart: 2, of which 0 were waited for; matrix products, arithmetic and copies ran while one was open for 2% of the time, Pallas kernels for 72%

profile of v2, /device:TPU:0, one launch (start us, length us, event | category | flops | bytes accessed | tf_op | source)
XLA Modules:
  0.0 149.6 jit_solution(12019236724930373127)
XLA Ops:
  7.2 0.0 copy-start
  7.2 0.0 reduce-scatter.2.cloned.1.call-start
  7.2 1.1 copy.28
  8.4 1.1 copy.29
  9.5 0.1 fusion.27
  9.6 4.9 %collective-permute-start = (bf16[128,128]{1,0:T(8,128)(2,1)S(1)}, bf16[128,128]{1,0:T(8,128)(2,1)S(1)}, u32[]{:S(2)}, u32[]{:S(2)}) collective-permute-start(bf16[128,128]{1,0:T(8,128)(2,1)S(1)} %fusion.27), channel_id=1, source_target_pairs={{0,4},{4,8},{8,12},{12,16},{16,20},{20,24},{24,28},{1,5},{5,9},{9,... | collective-permute-start | bytes 98312 | tf_op jit(solution)/shard_map/ppermute | solution.py:22
  14.5 0.1 iota_add_fusion
  14.6 0.5 fusion.17
  15.1 2.0 %reshape.148 = bf16[8,128,4,64]{3,2,1,0:T(4,128)(2,1)S(1)} reshape(bf16[1024,256]{1,0:T(8,128)(2,1)} %param.12) | data formatting | bytes 1048576 | tf_op jit(solution)/shard_map/reshape.2
  17.1 0.2 pad_maximum_fusion.1
  17.3 0.2 copy.30
  17.5 0.2 copy.31
  17.7 0.9 fusion.1
  18.6 0.1 broadcast_maximum_fusion
  18.7 1.0 fusion
  19.7 0.1 exponential_add_fusion
  19.8 1.2 fusion.8
  21.0 0.3 copy.35
  21.4 4.5 %fusion.18 = f32[1024,2048]{1,0:T(8,128)} fusion(bf16[256,2048]{1,0:T(8,128)(2,1)S(1)} %copy-done, bf16[32,8,8,128]{3,2,1,0:T(8,128)(2,1)S(1)} %bitcast.58), kind=kOutput, calls=%fused_computation.21 | convolution fusion | flops 1073741824 | bytes 9961472 | tf_op jit(solution)/shard_map/dot_general | solution.py:78
  25.9 0.0 reduce-scatter.2.cloned.1.call-update
  25.9 0.6 copy-done.7
  26.6 0.0 copy-done.8
  26.6 0.4 copy-done.4
  27.0 0.2 fusion.11
  27.2 0.2 fusion.13.rows_hbm
  27.4 1.6 %copy-done.1 = bf16[1,2048,512]{2,1,0:T(8,128)(2,1)S(1)} copy-done((bf16[1,2048,512]{2,1,0:T(8,128)(2,1)S(1)}, bf16[1,2048,512]{2,1,0:T(8,128)(2,1)}, u32[]{:S(2)}) %copy-start.1) | copy-done | bytes 2097176
  29.0 1.6 %copy-done.2 = bf16[1,2048,512]{2,1,0:T(8,128)(2,1)S(1)} copy-done((bf16[1,2048,512]{2,1,0:T(8,128)(2,1)S(1)}, bf16[1,2048,512]{2,1,0:T(8,128)(2,1)}, u32[]{:S(2)}) %copy-start.2) | copy-done | bytes 2097176
  30.6 1.6 %copy-done.3 = bf16[1,512,2048]{2,1,0:T(8,128)(2,1)S(1)} copy-done((bf16[1,512,2048]{2,1,0:T(8,128)(2,1)S(1)}, bf16[1,512,2048]{2,1,0:T(8,128)(2,1)}, u32[]{:S(2)}) %copy-start.3) | copy-done | bytes 2097176
  32.2 107.0 %shard_map.131 = bf16[128,2048]{1,0:T(8,128)(2,1)S(1)} custom-call(bf16[128,2048]{1,0:T(8,128)(2,1)S(1)} %fusion.13.rows_hbm, f32[8,128]{1,0:T(8,128)S(1)} %bitcast.54, bf16[2048,512]{1,0:T(8,128)(2,1)S(1)} %bitcast.55, bf16[2048,512]{1,0:T(8,128)(2,1)S(1)} %bitcast.56, bf16[512,2048]{1,0:T(8,128)(2,1)S(1)} %bitcast.57), custom_call_target="tpu_custom_call" | custom-call | flops 64424509440 | bytes 16777216 | tf_op jit(solution)/shard_map/pallas_call | solution.py:414
  139.2 0.0 reduce-scatter.2.cloned.1.call-done
  139.2 2.7 %convert_element_type.25 = bf16[256,2048]{1,0:T(8,128)(2,1)} convert(f32[256,2048]{1,0:T(8,128)} %reduce-scatter.2.cloned.1.call-done) | non-fusion elementwise | flops 524288 | bytes 3145728 | tf_op jit(solution)/shard_map/convert_element_type | solution.py:83
  141.9 0.8 copy.51
  (16 shorter events, 0.1 us)
Async XLA Ops:
  7.2 14.2 %copy-start = (bf16[256,2048]{1,0:T(8,128)(2,1)S(1)}, bf16[256,2048]{1,0:T(8,128)(2,1)}, u32[]{:S(2)}) copy-start(bf16[256,2048]{1,0:T(8,128)(2,1)} %param.16) | copy-start | bytes 3145732
  7.2 132.0 %reduce-scatter.2.cloned.1.call-start = ((), (), s32[]{:S(2)}) async-start(), calls=%async_computation.1 | async-start | bytes 10485760 | tf_op jit(solution)/shard_map/reduce_scatter | solution.py:77
  9.6 7.6 %collective-permute-start = (bf16[128,128]{1,0:T(8,128)(2,1)S(1)}, bf16[128,128]{1,0:T(8,128)(2,1)S(1)}, u32[]{:S(2)}, u32[]{:S(2)}) collective-permute-start(bf16[128,128]{1,0:T(8,128)(2,1)S(1)} %fusion.27), channel_id=1, source_target_pairs={{0,4},{4,8},{8,12},{12,16},{16,20},{20,24},{24,28},{1,5},{5,9},{9,... | collective-permute-start | bytes 98312 | tf_op jit(solution)/shard_map/ppermute | solution.py:22
  17.1 1.5 %copy-start.6 = (f32[4]{0:T(128)S(1)}, f32[4]{0:T(128)}, u32[]{:S(2)}) copy-start(f32[4]{0:T(128)} %param.15) | copy-start | bytes 52
  25.9 0.7 copy-start.7
  25.9 0.7 copy-start.8
  25.9 1.1 copy-start.4
  25.9 1.3 copy-start.5
  27.4 1.6 %copy-start.1 = (bf16[1,2048,512]{2,1,0:T(8,128)(2,1)S(1)}, bf16[1,2048,512]{2,1,0:T(8,128)(2,1)}, u32[]{:S(2)}) copy-start(bf16[1,2048,512]{2,1,0:T(8,128)(2,1)} %param.21) | copy-start | bytes 6291460
  29.0 1.6 %copy-start.2 = (bf16[1,2048,512]{2,1,0:T(8,128)(2,1)S(1)}, bf16[1,2048,512]{2,1,0:T(8,128)(2,1)}, u32[]{:S(2)}) copy-start(bf16[1,2048,512]{2,1,0:T(8,128)(2,1)} %param.22) | copy-start | bytes 6291460
  30.6 1.6 %copy-start.3 = (bf16[1,512,2048]{2,1,0:T(8,128)(2,1)S(1)}, bf16[1,512,2048]{2,1,0:T(8,128)(2,1)}, u32[]{:S(2)}) copy-start(bf16[1,512,2048]{2,1,0:T(8,128)(2,1)} %param.23) | copy-start | bytes 6291460
Sparse Core Ops, SparseCore 0:
  26.1 72.3 reduce-scatter.1

commit v3 on v2

--- a/solution.py
+++ b/solution.py
@@ -28,58 +28,77 @@
     return gate_cut * jax.nn.sigmoid(1.702 * gate_cut) * (up_cut + 1.0)
 
 
+def attention_kernel(seq_blocks, sinks, q_ref, k_ref, v_ref, edge_ref, weight_ref, out_ref):
+    block = pl.program_id(0)
+    local_kv = k_ref.shape[1] // HEAD_DIM
+    local_heads = q_ref.shape[1] // HEAD_DIM
+    per_group = local_heads // local_kv
+    key_width = local_kv * HEAD_DIM
+    opens = lax.rem(lax.axis_index("ep") * pl.num_programs(0) + block, seq_blocks) == 0
+    now = pl.ds(pl.multiple_of(block * WINDOW, WINDOW), WINDOW)
+    before = pl.ds(pl.multiple_of(jnp.maximum(block - 1, 0) * WINDOW, WINDOW), WINDOW)
+    edge = edge_ref[...]
+    keys = jnp.concatenate(
+        [jnp.where(block == 0, edge[:, :key_width], k_ref[before, :]), k_ref[now, :]], axis=0
+    )
+    values = jnp.concatenate(
+        [jnp.where(block == 0, edge[:, key_width:], v_ref[before, :]), v_ref[now, :]], axis=0
+    )
+    shape = (WINDOW, 2 * WINDOW)
+    column = lax.broadcasted_iota(jnp.int32, shape, 1)
+    distance = lax.broadcasted_iota(jnp.int32, shape, 0) + WINDOW - column
+    lowest = jnp.where(opens, WINDOW, 0)
+    valid = (distance >= 0) & (distance < WINDOW) & (column >= lowest)
+    outs = []
+    for head in range(local_heads):
+        group = head // per_group
+        span = slice(group * HEAD_DIM, (group + 1) * HEAD_DIM)
+        scores = lax.dot_general(
+            q_ref[:, head * HEAD_DIM : (head + 1) * HEAD_DIM],
+            keys[:, span],
+            (((1,), (1,)), ((), ())),
+            preferred_element_type=jnp.float32,
+        ) * HEAD_DIM ** (-0.5)
+        scores = jnp.where(valid, scores, NEGATIVE)
+        sink = sinks[head]
+        maxima = jnp.maximum(jnp.max(scores, axis=-1, keepdims=True), sink)
+        powers = jnp.exp(scores - maxima)
+        total = jnp.sum(powers, axis=-1, keepdims=True) + jnp.exp(sink - maxima)
+        weights = (powers / total).astype(jnp.bfloat16)
+        outs.append(jnp.dot(weights, values[:, span], preferred_element_type=jnp.float32))
+    heads_out = jnp.concatenate(outs, axis=1).astype(jnp.bfloat16)
+    out_ref[...] = jnp.dot(heads_out, weight_ref[...], preferred_element_type=jnp.float32)
+
+
 def attend(queries, head_keys, head_values, sink_logits, out_weight):
-    tok_rows = queries.shape[0]
-    local_heads = sink_logits.shape[0]
-    local_kv = head_keys.shape[1] // HEAD_DIM
-    per_group = local_heads // local_kv
-    block_count = tok_rows // WINDOW
-    key_width = local_kv * HEAD_DIM
-    kv_rows = jnp.concatenate([head_keys, head_values], axis=1)
-    earlier = passed_along(kv_rows[tok_rows - WINDOW :], "ep", 1)
-    extended = jnp.concatenate([earlier, kv_rows], axis=0)
-    banded = jnp.concatenate(
-        [
-            extended[:tok_rows].reshape(block_count, WINDOW, 2 * key_width),
-            kv_rows.reshape(block_count, WINDOW, 2 * key_width),
+    tok_rows, width = queries.shape
+    seq_len = tok_rows * lax.axis_size("ep") // SEQS
+    last = tok_rows - WINDOW
+    edge = passed_along(
+        jnp.concatenate([head_keys[last:], head_values[last:]], axis=1), "ep", 1
+    )
+    columns = out_weight.shape[1]
+    whole = lambda array: pl.BlockSpec(array.shape, lambda block: (0, 0))
+    partial = pl.pallas_call(
+        functools.partial(attention_kernel, seq_len // WINDOW),
+        grid=(tok_rows // WINDOW,),
+        out_shape=jax.ShapeDtypeStruct((tok_rows, columns), jnp.float32),
+        in_specs=[
+            pl.BlockSpec(memory_space=pltpu.SMEM),
+            pl.BlockSpec((WINDOW, width), lambda block: (block, 0)),
+            whole(head_keys),
+            whole(head_values),
+            whole(edge),
+            whole(out_weight),
         ],
-        axis=1,
-    )
-    band_keys = banded[:, :, :key_width].reshape(block_count, 2 * WINDOW, local_kv, HEAD_DIM)
-    band_values = banded[:, :, key_width:].reshape(block_count, 2 * WINDOW, local_kv, HEAD_DIM)
-    blocked = queries.reshape(block_count, WINDOW, local_kv, per_group, HEAD_DIM)
-    scores = jnp.einsum(
-        "nqkgd,nskd->nkgqs", blocked, band_keys, preferred_element_type=jnp.float32
-    ) * HEAD_DIM ** (-0.5)
-    offset = lax.axis_index("ep") * tok_rows
-    seq_len = tok_rows * lax.axis_size("ep") // SEQS
-    query_pos = offset + jnp.arange(tok_rows, dtype=jnp.int32).reshape(block_count, WINDOW)
-    key_pos = (
-        offset
-        - WINDOW
-        + (jnp.arange(block_count, dtype=jnp.int32) * WINDOW)[:, None]
-        + jnp.arange(2 * WINDOW, dtype=jnp.int32)[None, :]
-    )
-    distance = query_pos[:, :, None] - key_pos[:, None, :]
-    starts = query_pos // seq_len * seq_len
-    valid = (distance >= 0) & (distance < WINDOW) & (key_pos[:, None, :] >= starts[:, :, None])
-    scores = jnp.where(valid[:, None, None], scores, NEGATIVE)
-    sinks = sink_logits.reshape(local_kv, per_group, 1, 1)
-    maxima = jnp.maximum(jnp.max(scores, axis=-1, keepdims=True), sinks)
-    powers = jnp.exp(scores - maxima)
-    weights = (powers / (jnp.sum(powers, axis=-1, keepdims=True) + jnp.exp(sinks - maxima))).astype(
-        jnp.bfloat16
-    )
-    heads_out = jnp.einsum(
-        "nkgqs,nskd->nqkgd", weights, band_values, preferred_element_type=jnp.float32
-    )
-    heads_out = heads_out.astype(jnp.bfloat16).reshape(tok_rows, local_heads * HEAD_DIM)
-    summed = lax.psum_scatter(
-        jnp.dot(heads_out, out_weight, preferred_element_type=jnp.float32),
-        "tp",
-        scatter_dimension=0,
-        tiled=True,
-    )
+        out_specs=pl.BlockSpec((WINDOW, columns), lambda block: (block, 0)),
+        cost_estimate=pl.CostEstimate(
+            flops=4 * tok_rows * width * columns,
+            bytes_accessed=4 * tok_rows * columns,
+            transcendentals=0,
+        ),
+    )(sink_logits, queries, head_keys, head_values, edge, out_weight)
+    summed = lax.psum_scatter(partial, "tp", scatter_dimension=0, tiled=True)
     return summed.astype(jnp.bfloat16)
 
 

time: 150 us -> 152 us (1.013)
  Pallas kernels: 107 us -> 119 us
  matrix products: 6.63 us -> 0 us
  local copies, waits for them, and re-layouts: 11.6 us -> 8.19 us
  other arithmetic: 5.15 us -> 3.19 us
  waiting for transfers between devices: 0.04 us -> 1.62 us
    pallas_call x0 -> x1, Pallas kernels: none -> 12.7 us  [attend(): pl.pallas_call(functools.partial(attention_kernel, seq_len // WINDOW), gr...]
    dot_general x3 -> x0, matrix products: 6.63 us -> none  [the longest x1 4.51 us: attend(): jnp.dot(heads_out, out_weight, preferred_element_type=jnp.float32)]
    another operation x1 -> x0, local copies, waits for them, and re-layouts: 2.04 us -> none
    ppermute x1, waiting for transfers between devices: 0.01 us -> 1.58 us  [passed_along(): lax.ppermute(value, axis, [(source, source + steps) for source in range(f...]
    unnamed x21 -> x23, local copies, waits for them, and re-layouts: 8.84 us -> 8.18 us
  transfers between devices with their start and end apart: 2 -> 2, of which waited for: 0 -> 1; matrix products, arithmetic and copies ran while one was open for 2% -> 0% of each run, Pallas kernels for 72% -> 70%
where the time goes in v3:
time: 152 us; the launch traced here: 151 us
  Pallas kernels  119 us (78%)
  between operations  14.1 us (9%)
  local copies, waits for them, and re-layouts  8.19 us (5%)
  starting transfers between devices  4.94 us (3%)
  other arithmetic  3.19 us (2%)
  waiting for transfers between devices  1.62 us (1%)
    pallas_call x1, Pallas kernels, fused_experts(): pl.pallas_call(functools.partial(experts_kernel, count), out_shape=jax.Sh...  107 us
    pallas_call x1, Pallas kernels, attend(): pl.pallas_call(functools.partial(attention_kernel, seq_len // WINDOW), gr...  12.7 us
    unnamed x23, local copies, waits for them, and re-layouts  8.18 us
    ppermute x1, starting transfers between devices, passed_along(): lax.ppermute(value, axis, [(source, source + steps) for source in range(f...  4.9 us
  transfers between devices with their start and end apart: 2, of which 1 were waited for; matrix products, arithmetic and copies ran while one was open for 0% of the time, Pallas kernels for 70%

profile of v3, /device:TPU:0, one launch (start us, length us, event | category | flops | bytes accessed | tf_op | source)
XLA Modules:
  0.0 151.4 jit_solution(12123181245338069993)
XLA Ops:
  7.2 0.0 reduce-scatter.2.cloned.1.call-start
  7.2 1.1 copy.22.k_ref
  8.3 0.0 copy-start.4
  8.3 1.2 copy.23.v_ref
  9.5 0.0 copy-start.5
  9.5 0.1 pad_maximum_fusion
  9.6 4.9 %collective-permute-start = (bf16[128,128]{1,0:T(8,128)(2,1)S(1)}, bf16[128,128]{1,0:T(8,128)(2,1)S(1)}, u32[]{:S(2)}, u32[]{:S(2)}) collective-permute-start(bf16[128,128]{1,0:T(8,128)(2,1)S(1)} %pad_maximum_fusion), channel_id=1, source_target_pairs={{0,4},{4,8},{8,12},{12,16},{16,20},{20,24},{24,28},{1,5},{5,9},{9,... | collective-permute-start | bytes 98312 | tf_op jit(solution)/shard_map/ppermute | solution.py:22
  14.5 1.6 %collective-permute-done.edge_ref = bf16[128,128]{1,0:T(8,128)(2,1)S(1)} collective-permute-done((bf16[128,128]{1,0:T(8,128)(2,1)S(1)}, bf16[128,128]{1,0:T(8,128)(2,1)S(1)}, u32[]{:S(2)}, u32[]{:S(2)}) %collective-permute-start) | collective-permute-done | bytes 32800 | tf_op jit(solution)/shard_map/ppermute | solution.py:22
  16.1 0.0 copy-done.4
  16.1 0.0 copy-done.5
  16.1 0.0 copy-start.6
  16.1 0.6 copy-done.6
  16.7 12.7 %shard_map.131 = f32[1024,2048]{1,0:T(8,128)} custom-call(f32[4]{0:T(128)} %sinks.1, bf16[1024,256]{1,0:T(8,128)(2,1)} %q_ref.1, bf16[1024,64]{1,0:T(8,128)(2,1)} %copy-done.4, bf16[1024,64]{1,0:T(8,128)(2,1)} %copy-done.5, bf16[128,128]{1,0:T(8,128)(2,1)} %copy-done.6, bf16[256,2048]{1,0:T(8,128)(2,1)} %weight_ref.1), custom_call_target="tpu_custom_call" | custom-call | flops 2147483648 | bytes 8388608 | tf_op jit(solution)/shard_map/pallas_call | solution.py:82
  29.4 0.0 copy-start.8
  29.4 0.0 copy-start.9
  29.4 0.0 copy-start.7
  29.4 0.0 copy-start
  29.5 0.0 reduce-scatter.2.cloned.1.call-update
  29.5 0.6 copy-done.8
  30.1 0.0 copy-done.9
  30.1 0.4 copy-done.3
  30.5 0.2 fusion
  30.7 0.0 copy-done.7
  30.7 0.2 fusion.2.rows_hbm
  30.9 0.3 copy-done
  31.2 0.0 copy-start.1
  31.2 1.6 %copy-done.1 = bf16[1,2048,512]{2,1,0:T(8,128)(2,1)S(1)} copy-done((bf16[1,2048,512]{2,1,0:T(8,128)(2,1)S(1)}, bf16[1,2048,512]{2,1,0:T(8,128)(2,1)}, u32[]{:S(2)}) %copy-start.1) | copy-done | bytes 2097176
  32.8 1.6 %copy-done.2 = bf16[1,512,2048]{2,1,0:T(8,128)(2,1)S(1)} copy-done((bf16[1,512,2048]{2,1,0:T(8,128)(2,1)S(1)}, bf16[1,512,2048]{2,1,0:T(8,128)(2,1)}, u32[]{:S(2)}) %copy-start.2) | copy-done | bytes 2097176
  34.4 106.5 %shard_map.132 = bf16[128,2048]{1,0:T(8,128)(2,1)S(1)} custom-call(bf16[128,2048]{1,0:T(8,128)(2,1)S(1)} %fusion.2.rows_hbm, f32[8,128]{1,0:T(8,128)S(1)} %bitcast.4, bf16[2048,512]{1,0:T(8,128)(2,1)S(1)} %bitcast.5, bf16[2048,512]{1,0:T(8,128)(2,1)S(1)} %bitcast.6, bf16[512,2048]{1,0:T(8,128)(2,1)S(1)} %bitcast.7), custom_call_target="tpu_custom_call" | custom-call | flops 64424509440 | bytes 16777216 | tf_op jit(solution)/shard_map/pallas_call | solution.py:433
  141.0 0.0 reduce-scatter.2.cloned.1.call-done
  141.0 2.7 %convert_element_type.9 = bf16[256,2048]{1,0:T(8,128)(2,1)} convert(f32[256,2048]{1,0:T(8,128)} %reduce-scatter.2.cloned.1.call-done) | non-fusion elementwise | flops 524288 | bytes 3145728 | tf_op jit(solution)/shard_map/convert_element_type | solution.py:102
  143.7 0.8 copy.25
  (6 shorter events, 0.0 us)
Async XLA Ops:
  7.2 133.8 %reduce-scatter.2.cloned.1.call-start = ((), (), s32[]{:S(2)}) async-start(), calls=%async_computation.1 | async-start | bytes 10485760 | tf_op jit(solution)/shard_map/reduce_scatter | solution.py:101
  8.3 7.8 %copy-start.4 = (bf16[1024,64]{1,0:T(8,128)(2,1)}, bf16[1024,64]{1,0:T(8,128)(2,1)S(1)}, u32[]{:S(2)}) copy-start(bf16[1024,64]{1,0:T(8,128)(2,1)S(1)} %copy.22.k_ref) | copy-start | bytes 393220
  9.5 6.6 %copy-start.5 = (bf16[1024,64]{1,0:T(8,128)(2,1)}, bf16[1024,64]{1,0:T(8,128)(2,1)S(1)}, u32[]{:S(2)}) copy-start(bf16[1024,64]{1,0:T(8,128)(2,1)S(1)} %copy.23.v_ref) | copy-start | bytes 393220
  9.6 6.5 %collective-permute-start = (bf16[128,128]{1,0:T(8,128)(2,1)S(1)}, bf16[128,128]{1,0:T(8,128)(2,1)S(1)}, u32[]{:S(2)}, u32[]{:S(2)}) collective-permute-start(bf16[128,128]{1,0:T(8,128)(2,1)S(1)} %pad_maximum_fusion), channel_id=1, source_target_pairs={{0,4},{4,8},{8,12},{12,16},{16,20},{20,24},{24,28},{1,5},{5,9},{9,... | collective-permute-start | bytes 98312 | tf_op jit(solution)/shard_map/ppermute | solution.py:22
  16.1 0.6 copy-start.6
  29.4 0.7 copy-start.8
  29.4 0.7 copy-start.9
  29.4 1.1 copy-start.3
  29.4 1.3 copy-start.7
  29.4 1.8 %copy-start = (bf16[1,2048,512]{2,1,0:T(8,128)(2,1)S(1)}, bf16[1,2048,512]{2,1,0:T(8,128)(2,1)}, u32[]{:S(2)}) copy-start(bf16[1,2048,512]{2,1,0:T(8,128)(2,1)} %param.21) | copy-start | bytes 6291460
  31.2 1.6 %copy-start.1 = (bf16[1,2048,512]{2,1,0:T(8,128)(2,1)S(1)}, bf16[1,2048,512]{2,1,0:T(8,128)(2,1)}, u32[]{:S(2)}) copy-start(bf16[1,2048,512]{2,1,0:T(8,128)(2,1)} %param.22) | copy-start | bytes 6291460
  32.8 1.6 %copy-start.2 = (bf16[1,512,2048]{2,1,0:T(8,128)(2,1)S(1)}, bf16[1,512,2048]{2,1,0:T(8,128)(2,1)}, u32[]{:S(2)}) copy-start(bf16[1,512,2048]{2,1,0:T(8,128)(2,1)} %param.23) | copy-start | bytes 6291460
Sparse Core Ops, SparseCore 0:
  29.6 73.4 reduce-scatter.1
